TPU v7x, 32 devices: a whole 2x2x4 slice. The times are simulated.
32 devices in a mesh: fs: 8 (over z, y), tp: 4 (over x, core).
Axes of the slice: x: 2, y: 2, z: 4, core: 2. Of those that a mesh axis runs over, the one named last changes fastest.
Arguments:
- weights_in: float32 [2, 2048, 5632], P(None, 'fs', 'tp'), may hold values from -6 to 6
- weights_mix: float32 [2048, 2048], P('fs', 'tp'), may hold values from -6 to 6
- momentum_in: float32 [2, 2048, 5632], P(None, 'fs', 'tp'), may hold values from -5 to 5
- momentum_mix: float32 [2048, 2048], P('fs', 'tp'), may hold values from -5 to 5
- grads_in: float32 [2, 2048, 5632], P(None, 'fs', 'tp'), may hold values from -5 to 5
- grads_mix: float32 [2048, 2048], P('fs', 'tp'), may hold values from -5 to 5
Outputs:
- momentum_in_next: float32 [2, 2048, 5632], P(None, 'fs', 'tp')
- momentum_mix_next: float32 [2048, 2048], P('fs', 'tp')
- weights_in_next: float32 [2, 2048, 5632], P(None, 'fs', 'tp')
- weights_mix_next: float32 [2048, 2048], P('fs', 'tp')
- update_in: float32 [2, 2048, 5632], P(None, 'fs', 'tp')
- update_mix: float32 [2048, 2048], P('fs', 'tp')
All inputs are finite; a program needn't handle non-finite values.
Results may differ from a plain program's by a relative error of at most 0.0003.
Values sent between devices are 32-bit elements; how exact they have to be, the bound alone decides.
A program may use at most 128 MiB of HBM per device.

v0:
```python
import math
import jax
import jax.numpy as jnp
from jax import lax
from jax.sharding import PartitionSpec as P

D = 2048
FF = 5632
ITERS = 3
A_COEF = 3.4445
B_COEF = -4.775
C_COEF = 2.0315
MOMENTUM_DECAY = 0.95
STEP_RATE = 0.02
HIGH = lax.Precision.HIGHEST


def row_squares(shard):
    return jnp.sum(jnp.square(shard), axis=(1, 2))


def scale_from(summed):
    return (0.5 * lax.rsqrt(jnp.maximum(summed / D, 1.0)))[:, None, None]


def local(weights_in, weights_mix, momentum_in, momentum_mix, grads_in, grads_mix):
    moment_in = MOMENTUM_DECAY * momentum_in + grads_in
    moment_mix = MOMENTUM_DECAY * momentum_mix + grads_mix
    local_in = moment_in
    local_mix = moment_mix[None]
    squares = jnp.concatenate([row_squares(local_in), row_squares(local_mix)])
    scaling = scale_from(lax.psum(squares, ("fs", "tp")))
    for iteration in range(ITERS):
        cols_in, cols_mix = (
            lax.all_gather(local_in, "fs", axis=1, tiled=True),
            lax.all_gather(local_mix, "fs", axis=1, tiled=True),
        )
        partial_value = jnp.concatenate(
            [
                jnp.einsum("krc,ksc->krs", local_in, cols_in, precision=HIGH),
                jnp.einsum("krc,ksc->krs", local_mix, cols_mix, precision=HIGH),
            ]
        )
        gram_block = lax.psum_scatter(partial_value, "tp", scatter_dimension=2, tiled=True)
        gram_rows = lax.all_gather(gram_block, "tp", axis=2, tiled=True)
        factor = scaling if iteration == 0 else jnp.ones_like(scaling)
        gram_cols = lax.all_gather(gram_block, "fs", axis=1, tiled=True)
        square = jnp.einsum("krs,ksc->krc", gram_rows, gram_cols, precision=HIGH)
        poly_mat = factor**2 * B_COEF * gram_block + factor**4 * C_COEF * square
        poly_rows = lax.all_gather(poly_mat, "tp", axis=2, tiled=True)
        local_in = factor[:2] * (
            A_COEF * local_in + jnp.einsum("krs,ksc->krc", poly_rows[:2], cols_in, precision=HIGH)
        )
        local_mix = factor[2:] * (
            A_COEF * local_mix + jnp.einsum("krs,ksc->krc", poly_rows[2:], cols_mix, precision=HIGH)
        )
    step_in = local_in * math.sqrt(max(D, FF))
    step_mix = local_mix[0] * math.sqrt(D)
    return (
        moment_in,
        moment_mix,
        weights_in - STEP_RATE * step_in,
        weights_mix - STEP_RATE * step_mix,
        step_in,
        step_mix,
    )


def solution(mesh):
    in_specs = (
        P(None, "fs", "tp"),
        P("fs", "tp"),
        P(None, "fs", "tp"),
        P("fs", "tp"),
        P(None, "fs", "tp"),
        P("fs", "tp"),
    )
    out_specs = (
        P(None, "fs", "tp"),
        P("fs", "tp"),
        P(None, "fs", "tp"),
        P("fs", "tp"),
        P(None, "fs", "tp"),
        P("fs", "tp"),
    )
    return jax.shard_map(local, mesh=mesh, in_specs=in_specs, out_specs=out_specs, check_vma=False)
```

profile of v0, /device:TPU:0, one launch (start us, length us, event | category | flops | bytes accessed | tf_op | source)
XLA Modules:
  0.0 2754.7 jit_solution(12206210918786785973)
XLA Ops:
  7.2 2.7 multiply_reduce_fusion.1
  10.0 4.7 multiply_reduce_fusion
  14.7 71.5 %all-gather.43.cloned.1.call-done = f32[2048,512]{1,0:T(8,128)} async-done(((f32[256,512]{1,0:T(8,128)}), f32[2048,512]{1,0:T(8,128)}) %all-gather.43.cloned.1.call-update) | async-done | bytes 4194320 | tf_op jit(solution)/shard_map/all_gather | solution.py:36
  86.2 7.1 convolution_bitcast_fusion.2
  93.4 434.6 %all-gather.19.cloned.1.call-done = f32[2,2048,1408]{2,1,0:T(8,128)} async-done(((f32[2,256,1408]{2,1,0:T(8,128)}), f32[2,2048,1408]{2,1,0:T(8,128)}) %all-gather.19.cloned.1.call-update) | async-done | bytes 23068688 | tf_op jit(solution)/shard_map/all_gather | solution.py:35
  528.0 24.5 fusion.8
  552.5 3.1 pad_maximum_fusion
  555.7 58.0 %reduce-scatter.4.cloned.1.call-done = f32[3,256,512]{2,1,0:T(8,128)} async-done(((f32[3,256,2048]{2,1,0:T(8,128)}), f32[3,256,512]{2,1,0:T(8,128)}) %reduce-scatter.4.cloned.1.call-update) | async-done | bytes 1572880 | tf_op jit(solution)/shard_map/reduce_scatter | solution.py:44
  613.7 0.5 all-gather.23.cloned.1.call-update
  614.3 0.7 pad_maximum_fusion.3
  615.0 40.5 %psum.7 = f32[3]{0:T(128)S(1)} all-reduce(f32[3]{0:T(128)S(1)} %pad_maximum_fusion.3), channel_id=1, replica_groups=mesh['fs'=8,'tp'=4] {'fs','tp'}, use_global_device_ids=true, to_apply=%region_2.0 | all-reduce | flops 3 | bytes 24 | tf_op jit(solution)/shard_map/psum | solution.py:32
  655.6 6.8 all-gather.21.cloned.1.call-done
  662.3 178.2 %all-gather.23.cloned.1.call-done = f32[3,2048,512]{2,1,0:T(8,128)} async-done(((f32[3,256,512]{2,1,0:T(8,128)}), f32[3,2048,512]{2,1,0:T(8,128)}) %all-gather.23.cloned.1.call-update) | async-done | bytes 12582928 | tf_op jit(solution)/shard_map/all_gather | solution.py:47
  840.5 17.5 multiply_add_fusion.3
  858.1 0.6 slice.28
  858.7 44.1 %all-gather.25.cloned.1.call-done = f32[3,256,2048]{2,1,0:T(8,128)} async-done(((f32[3,256,512]{2,1,0:T(8,128)}), f32[3,256,2048]{2,1,0:T(8,128)}) %all-gather.25.cloned.1.call-update) | async-done | bytes 6291472 | tf_op jit(solution)/shard_map/all_gather | solution.py:50
  902.7 8.0 fusion.5
  910.7 0.6 all-gather.27.cloned.1.call-start
  911.3 27.5 fusion
  939.0 44.6 %all-gather.45.cloned.1.call-done = f32[2048,512]{1,0:T(8,128)} async-done(((f32[256,512]{1,0:T(8,128)}), f32[2048,512]{1,0:T(8,128)}) %all-gather.45.cloned.1.call-update) | async-done | bytes 4194320 | tf_op jit(solution)/shard_map/all_gather | solution.py:36
  983.7 7.1 convolution_bitcast_fusion.1
  990.8 434.6 %all-gather.27.cloned.1.call-done = f32[2,2048,1408]{2,1,0:T(8,128)} async-done(((f32[2,256,1408]{2,1,0:T(8,128)}), f32[2,2048,1408]{2,1,0:T(8,128)}) %all-gather.27.cloned.1.call-update) | async-done | bytes 23068688 | tf_op jit(solution)/shard_map/all_gather | solution.py:35
  1425.4 24.5 fusion.9
  1449.9 3.1 pad_maximum_fusion.1
  1453.1 58.0 %reduce-scatter.6.cloned.1.call-done = f32[3,256,512]{2,1,0:T(8,128)} async-done(((f32[3,256,2048]{2,1,0:T(8,128)}), f32[3,256,512]{2,1,0:T(8,128)}) %reduce-scatter.6.cloned.1.call-update) | async-done | bytes 1572880 | tf_op jit(solution)/shard_map/reduce_scatter | solution.py:44
  1511.2 0.7 all-gather.31.cloned.1.call-update
  1511.9 0.3 all-gather.33.cloned.1.call-start
  1512.1 46.8 %all-gather.29.cloned.1.call-done = f32[3,256,2048]{2,1,0:T(8,128)} async-done(((f32[3,256,512]{2,1,0:T(8,128)}), f32[3,256,2048]{2,1,0:T(8,128)}) %all-gather.29.cloned.1.call-update) | async-done | bytes 6291472 | tf_op jit(solution)/shard_map/all_gather | solution.py:45
  1558.9 178.3 %all-gather.31.cloned.1.call-done = f32[3,2048,512]{2,1,0:T(8,128)} async-done(((f32[3,256,512]{2,1,0:T(8,128)}), f32[3,2048,512]{2,1,0:T(8,128)}) %all-gather.31.cloned.1.call-update) | async-done | bytes 12582928 | tf_op jit(solution)/shard_map/all_gather | solution.py:47
  1737.2 17.5 multiply_add_fusion.2
  1754.8 44.6 %all-gather.33.cloned.1.call-done = f32[3,256,2048]{2,1,0:T(8,128)} async-done(((f32[3,256,512]{2,1,0:T(8,128)}), f32[3,256,2048]{2,1,0:T(8,128)}) %all-gather.33.cloned.1.call-update) | async-done | bytes 6291472 | tf_op jit(solution)/shard_map/all_gather | solution.py:50
  1799.5 7.3 fusion.6
  1806.8 0.3 all-gather.35.cloned.1.call-start
  1807.1 27.4 convolution_add_fusion.1
  1834.5 0.5 reduce-scatter.8.cloned.1.call-start
  1835.0 44.7 %all-gather.47.cloned.1.call-done = f32[2048,512]{1,0:T(8,128)} async-done(((f32[256,512]{1,0:T(8,128)}), f32[2048,512]{1,0:T(8,128)}) %all-gather.47.cloned.1.call-update) | async-done | bytes 4194320 | tf_op jit(solution)/shard_map/all_gather | solution.py:36
  1879.7 7.1 convolution_bitcast_fusion
  1886.9 434.4 %all-gather.35.cloned.1.call-done = f32[2,2048,1408]{2,1,0:T(8,128)} async-done(((f32[2,256,1408]{2,1,0:T(8,128)}), f32[2,2048,1408]{2,1,0:T(8,128)}) %all-gather.35.cloned.1.call-update) | async-done | bytes 23068688 | tf_op jit(solution)/shard_map/all_gather | solution.py:35
  2321.3 24.5 fusion.10
  2345.9 3.1 pad_maximum_fusion.2
  2349.1 58.0 %reduce-scatter.8.cloned.1.call-done = f32[3,256,512]{2,1,0:T(8,128)} async-done(((f32[3,256,2048]{2,1,0:T(8,128)}), f32[3,256,512]{2,1,0:T(8,128)}) %reduce-scatter.8.cloned.1.call-update) | async-done | bytes 1572880 | tf_op jit(solution)/shard_map/reduce_scatter | solution.py:44
  2407.1 0.5 all-gather.39.cloned.1.call-update
  2407.9 47.0 %all-gather.37.cloned.1.call-done = f32[3,256,2048]{2,1,0:T(8,128)} async-done(((f32[3,256,512]{2,1,0:T(8,128)}), f32[3,256,2048]{2,1,0:T(8,128)}) %all-gather.37.cloned.1.call-update) | async-done | bytes 6291472 | tf_op jit(solution)/shard_map/all_gather | solution.py:45
  2454.8 178.2 %all-gather.39.cloned.1.call-done = f32[3,2048,512]{2,1,0:T(8,128)} async-done(((f32[3,256,512]{2,1,0:T(8,128)}), f32[3,2048,512]{2,1,0:T(8,128)}) %all-gather.39.cloned.1.call-update) | async-done | bytes 12582928 | tf_op jit(solution)/shard_map/all_gather | solution.py:47
  2633.0 17.5 multiply_add_fusion.1
  2650.5 44.7 %all-gather.41.cloned.1.call-done = f32[3,256,2048]{2,1,0:T(8,128)} async-done(((f32[3,256,512]{2,1,0:T(8,128)}), f32[3,256,2048]{2,1,0:T(8,128)}) %all-gather.41.cloned.1.call-update) | async-done | bytes 6291472 | tf_op jit(solution)/shard_map/all_gather | solution.py:50
  2695.2 46.1 %broadcast_multiply_fusion = (f32[2,256,1408]{2,1,0:T(8,128)}, f32[2,256,1408]{2,1,0:T(8,128)}) fusion(f32[2,256,1408]{2,1,0:T(8,128)} %param.6, f32[3,256,2048]{2,1,0:T(8,128)} %all-gather.41.cloned.1.call-done, f32[2,2048,1408]{2,1,0:T(8,128)} %all-gather.35.cloned.1.call-done, f32[2,256,1408]{2,1,0:T(8,128)S(1)} %copy-done.2), kind=kOutput, calls=%fused_computation.22 | convolution fusion | flops 17720344576 | bytes 40894464 | tf_op jit(solution)/shard_map/krs,ksc->krc/dot_general | solution.py:52
  2741.3 6.3 broadcast_multiply_fusion.1
  (53 shorter events, 1.2 us)
Async XLA Ops:
  7.2 79.1 %all-gather.43.cloned.1.call-start = ((), (), s32[]{:S(2)}) async-start(), calls=%async_computation.18 | async-start | bytes 4718592 | tf_op jit(solution)/shard_map/all_gather | solution.py:36
  9.9 76.3 %copy-start.9 = (f32[256,512]{1,0:T(8,128)S(1)}, f32[256,512]{1,0:T(8,128)}, u32[]{:S(2)}) copy-start(f32[256,512]{1,0:T(8,128)} %get-tuple-element.11) | copy-start | bytes 1572868
  9.9 518.0 %all-gather.19.cloned.1.call-start = ((), (), s32[]{:S(2)}) async-start(), calls=%async_computation.3 | async-start | bytes 25952256 | tf_op jit(solution)/shard_map/all_gather | solution.py:35
  14.7 513.3 %copy-start = (f32[2,256,1408]{2,1,0:T(8,128)S(1)}, f32[2,256,1408]{2,1,0:T(8,128)}, u32[]{:S(2)}) copy-start(f32[2,256,1408]{2,1,0:T(8,128)} %get-tuple-element.9) | copy-start | bytes 8650756
  14.7 599.0 %reduce-scatter.4.cloned.1.call-start = ((), (), s32[]{:S(2)}) async-start(), calls=%async_computation.4 | async-start | bytes 7864320 | tf_op jit(solution)/shard_map/reduce_scatter | solution.py:44
  528.0 24.6 copy-start.6
  555.6 106.7 %all-gather.21.cloned.1.call-start = ((), (), s32[]{:S(2)}) async-start(), calls=%async_computation.5 | async-start | bytes 7864320 | tf_op jit(solution)/shard_map/all_gather | solution.py:45
  613.7 226.8 %all-gather.23.cloned.1.call-start = ((), (), s32[]{:S(2)}) async-start(), calls=%async_computation.6 | async-start | bytes 14155776 | tf_op jit(solution)/shard_map/all_gather | solution.py:47
  614.3 288.5 %all-gather.25.cloned.1.call-start = ((), (), s32[]{:S(2)}) async-start(), calls=%async_computation.7 | async-start | bytes 7864320 | tf_op jit(solution)/shard_map/all_gather | solution.py:50
  858.0 125.6 %all-gather.45.cloned.1.call-start = ((), (), s32[]{:S(2)}) async-start(), calls=%async_computation.19 | async-start | bytes 4718592 | tf_op jit(solution)/shard_map/all_gather | solution.py:36
  910.7 514.7 %all-gather.27.cloned.1.call-start = ((), (), s32[]{:S(2)}) async-start(), calls=%async_computation.8 | async-start | bytes 25952256 | tf_op jit(solution)/shard_map/all_gather | solution.py:35
  911.3 72.4 %copy-start.5 = (f32[256,512]{1,0:T(8,128)S(1)}, f32[256,512]{1,0:T(8,128)}, u32[]{:S(2)}) copy-start(f32[256,512]{1,0:T(8,128)} %fusion.5) | copy-start | bytes 1572868
  938.8 486.6 %copy-start.1 = (f32[2,256,1408]{2,1,0:T(8,128)S(1)}, f32[2,256,1408]{2,1,0:T(8,128)}, u32[]{:S(2)}) copy-start(f32[2,256,1408]{2,1,0:T(8,128)} %fusion) | copy-start | bytes 8650756
  938.8 572.3 %reduce-scatter.6.cloned.1.call-start = ((), (), s32[]{:S(2)}) async-start(), calls=%async_computation.9 | async-start | bytes 7864320 | tf_op jit(solution)/shard_map/reduce_scatter | solution.py:44
  1425.4 24.6 copy-start.7
  1453.1 105.8 %all-gather.29.cloned.1.call-start = ((), (), s32[]{:S(2)}) async-start(), calls=%async_computation.10 | async-start | bytes 7864320 | tf_op jit(solution)/shard_map/all_gather | solution.py:45
  1511.1 226.1 %all-gather.31.cloned.1.call-start = ((), (), s32[]{:S(2)}) async-start(), calls=%async_computation.11 | async-start | bytes 14155776 | tf_op jit(solution)/shard_map/all_gather | solution.py:47
  1511.9 287.6 %all-gather.33.cloned.1.call-start = ((), (), s32[]{:S(2)}) async-start(), calls=%async_computation.12 | async-start | bytes 7864320 | tf_op jit(solution)/shard_map/all_gather | solution.py:50
  1754.8 125.0 %all-gather.47.cloned.1.call-start = ((), (), s32[]{:S(2)}) async-start(), calls=%async_computation.20 | async-start | bytes 4718592 | tf_op jit(solution)/shard_map/all_gather | solution.py:36
  1806.8 73.0 %copy-start.4 = (f32[256,512]{1,0:T(8,128)S(1)}, f32[256,512]{1,0:T(8,128)}, u32[]{:S(2)}) copy-start(f32[256,512]{1,0:T(8,128)} %fusion.6) | copy-start | bytes 1572868
  1806.8 514.5 %all-gather.35.cloned.1.call-start = ((), (), s32[]{:S(2)}) async-start(), calls=%async_computation.13 | async-start | bytes 25952256 | tf_op jit(solution)/shard_map/all_gather | solution.py:35
  1834.5 486.8 %copy-start.2 = (f32[2,256,1408]{2,1,0:T(8,128)S(1)}, f32[2,256,1408]{2,1,0:T(8,128)}, u32[]{:S(2)}) copy-start(f32[2,256,1408]{2,1,0:T(8,128)} %convolution_add_fusion.1) | copy-start | bytes 8650756
  1834.5 572.5 %reduce-scatter.8.cloned.1.call-start = ((), (), s32[]{:S(2)}) async-start(), calls=%async_computation.14 | async-start | bytes 7864320 | tf_op jit(solution)/shard_map/reduce_scatter | solution.py:44
  2321.3 24.6 copy-start.8
  2349.0 105.8 %all-gather.37.cloned.1.call-start = ((), (), s32[]{:S(2)}) async-start(), calls=%async_computation.15 | async-start | bytes 7864320 | tf_op jit(solution)/shard_map/all_gather | solution.py:45
  2407.0 225.9 %all-gather.39.cloned.1.call-start = ((), (), s32[]{:S(2)}) async-start(), calls=%async_computation.16 | async-start | bytes 14155776 | tf_op jit(solution)/shard_map/all_gather | solution.py:47
  2407.6 287.6 %all-gather.41.cloned.1.call-start = ((), (), s32[]{:S(2)}) async-start(), calls=%async_computation.17 | async-start | bytes 7864320 | tf_op jit(solution)/shard_map/all_gather | solution.py:50
  2695.2 46.1 %copy-start.3 = (f32[2048,512]{1,0:T(8,128)S(1)}, f32[2048,512]{1,0:T(8,128)}, u32[]{:S(2)}) copy-start(f32[2048,512]{1,0:T(8,128)} %all-gather.47.cloned.1.call-done) | copy-start | bytes 12582916
  2695.2 46.1 %copy-start.10 = (f32[256,512]{1,0:T(8,128)S(1)}, f32[256,512]{1,0:T(8,128)}, u32[]{:S(2)}) copy-start(f32[256,512]{1,0:T(8,128)} %param.7) | copy-start | bytes 1572868
Sparse Core Ops, SparseCore 0:
  10.7 75.5 all-gather.42
  88.3 439.5 all-gather.18
  555.8 57.8 reduce-scatter.3
  615.1 47.2 all-gather.20
  664.4 176.0 all-gather.22
  858.2 44.5 all-gather.24
  910.8 72.7 all-gather.44
  985.8 439.5 all-gather.26
  1453.2 57.8 reduce-scatter.5
  1512.5 46.3 all-gather.28
  1561.1 176.0 all-gather.30
  1754.9 44.5 all-gather.32
  1806.9 72.7 all-gather.46
  1881.7 439.5 all-gather.34
  2349.1 57.8 reduce-scatter.7
  2408.4 46.3 all-gather.36
  2456.8 176.0 all-gather.38
  2650.7 44.5 all-gather.40
where the time goes:
time: 2760 us; the launch traced here: 2750 us
  waiting for transfers between devices  2410 us (87%)
  matrix products  270 us (10%)
  blocking collectives  40.5 us (1%)
    all_gather x3, waiting for transfers between devices, local(): lax.all_gather(local_in, 'fs', axis=1, tiled=True)  1300 us
    all_gather x3, waiting for transfers between devices, local(): gram_cols = lax.all_gather(gram_block, 'fs', axis=1, tiled=True)  535 us
    reduce_scatter x3, waiting for transfers between devices, local(): lax.psum_scatter(partial_value, 'tp', scatter_dimension=2, tiled=True)  174 us
    all_gather x3, waiting for transfers between devices, local(): lax.all_gather(local_mix, 'fs', axis=1, tiled=True)  161 us
    all_gather x3, waiting for transfers between devices, local(): poly_rows = lax.all_gather(poly_mat, 'tp', axis=2, tiled=True)  133 us
    dot_general x3, matrix products, local(): jnp.einsum('krs,ksc->krc', poly_rows[:2], cols_in, precision=HIGH)  101 us
    all_gather x3, waiting for transfers between devices, local(): gram_rows = lax.all_gather(gram_block, 'tp', axis=2, tiled=True)  100 us
    dot_general x3, matrix products, local(): jnp.einsum('krc,ksc->krs', local_in, cols_in, precision=HIGH)  73.6 us
  transfers between devices with their start and end apart: 18, of which 18 were waited for; matrix products, arithmetic and copies ran while one was open for 3% of the time, Pallas kernels for 0%

commit v1 on v0

--- a/solution.py
+++ b/solution.py
@@ -44,8 +44,31 @@
         gram_block = lax.psum_scatter(partial_value, "tp", scatter_dimension=2, tiled=True)
         gram_rows = lax.all_gather(gram_block, "tp", axis=2, tiled=True)
         factor = scaling if iteration == 0 else jnp.ones_like(scaling)
-        gram_cols = lax.all_gather(gram_block, "fs", axis=1, tiled=True)
-        square = jnp.einsum("krs,ksc->krc", gram_rows, gram_cols, precision=HIGH)
+
+        def draft_lanes_on_mesh(arr, chip_axis, incoming_x):
+            y1 = lax.axis_index(chip_axis)
+            after = lax.axis_size(chip_axis)
+            b_next, inter = (after, y1)
+            slots = [(jj, (jj - 1) % b_next) for jj in range(b_next)]
+            side_arr = arr.shape[1]
+            new = arr
+            view_out = incoming_x(new, inter * side_arr)
+            for dev_i in range(1, b_next):
+                new = lax.ppermute(new, chip_axis, slots)
+                back = incoming_x(new, (inter + dev_i) % b_next * side_arr)
+                view_out = view_out + back
+            return view_out
+
+        square = draft_lanes_on_mesh(
+            gram_block,
+            "fs",
+            lambda part, at: jnp.einsum(
+                "krs,ksc->krc",
+                lax.dynamic_slice_in_dim(gram_rows, at, part.shape[1], axis=2),
+                part,
+                precision=HIGH,
+            ),
+        )
         poly_mat = factor**2 * B_COEF * gram_block + factor**4 * C_COEF * square
         poly_rows = lax.all_gather(poly_mat, "tp", axis=2, tiled=True)
         local_in = factor[:2] * (

time: 2760 us -> 2850 us (1.033)
  starting transfers between devices: 2.52 us -> 106 us
  waiting for transfers between devices: 2410 us -> 2360 us
    ppermute x0 -> x21, waiting for transfers between devices: none -> 579 us  [draft_lanes_on_mesh(): new = lax.ppermute(new, chip_axis, slots)]
    all_gather x3 -> x0, waiting for transfers between devices: 535 us -> none  [local(): gram_cols = lax.all_gather(gram_block, 'fs', axis=1, tiled=True)]
    ppermute x0 -> x21, starting transfers between devices: none -> 104 us  [draft_lanes_on_mesh(): new = lax.ppermute(new, chip_axis, slots)]
    all_gather x3, waiting for transfers between devices: 100 us -> 0.02 us  [local(): gram_rows = lax.all_gather(gram_block, 'tp', axis=2, tiled=True)]
    dot_general x3 -> x24, matrix products: 52.6 us -> 63.2 us  [local(): jnp.einsum('krs,ksc->krc', lax.dynamic_slice_in_dim(gram_rows, at, part.s...]
  transfers between devices with their start and end apart: 18 -> 36, of which waited for: 18 -> 32; matrix products, arithmetic and copies ran while one was open for 3% -> 5% of each run, Pallas kernels for 0% -> 0%
where the time goes in v1:
time: 2850 us
  waiting for transfers between devices  2360 us (83%)
  matrix products  272 us (10%)
  starting transfers between devices  106 us (4%)
  blocking collectives  63.7 us (2%)
    all_gather x3, waiting for transfers between devices, local(): lax.all_gather(local_in, 'fs', axis=1, tiled=True)  1300 us
    ppermute x21, waiting for transfers between devices, draft_lanes_on_mesh(): new = lax.ppermute(new, chip_axis, slots)  579 us
    reduce_scatter x3, waiting for transfers between devices, local(): lax.psum_scatter(partial_value, 'tp', scatter_dimension=2, tiled=True)  174 us
    all_gather x3, waiting for transfers between devices, local(): lax.all_gather(local_mix, 'fs', axis=1, tiled=True)  162 us
    all_gather x3, waiting for transfers between devices, local(): poly_rows = lax.all_gather(poly_mat, 'tp', axis=2, tiled=True)  142 us
    ppermute x21, starting transfers between devices, draft_lanes_on_mesh(): new = lax.ppermute(new, chip_axis, slots)  104 us
    dot_general x3, matrix products, local(): jnp.einsum('krs,ksc->krc', poly_rows[:2], cols_in, precision=HIGH)  89.9 us
    dot_general x3, matrix products, local(): jnp.einsum('krc,ksc->krs', local_in, cols_in, precision=HIGH)  73.6 us
  transfers between devices with their start and end apart: 36, of which 32 were waited for; matrix products, arithmetic and copies ran while one was open for 5% of the time, Pallas kernels for 0%

profile of v1, /device:TPU:0, one launch (start us, length us, event | category | flops | bytes accessed | tf_op | source)
XLA Modules:
  0.0 2846.2 jit_solution(2088919258547041636)
XLA Ops:
  14.7 71.5 %all-gather.34.cloned.1.call-done = f32[2048,512]{1,0:T(8,128)} async-done(((f32[256,512]{1,0:T(8,128)}), f32[2048,512]{1,0:T(8,128)}) %all-gather.34.cloned.1.call-update) | async-done | bytes 4194320 | tf_op jit(solution)/shard_map/all_gather | solution.py:36
  86.2 7.3 convolution_bitcast_fusion.2
  93.5 434.4 %all-gather.16.cloned.1.call-done = f32[2,2048,1408]{2,1,0:T(8,128)} async-done(((f32[2,256,1408]{2,1,0:T(8,128)}), f32[2,2048,1408]{2,1,0:T(8,128)}) %all-gather.16.cloned.1.call-update) | async-done | bytes 23068688 | tf_op jit(solution)/shard_map/all_gather | solution.py:35
  528.0 24.5 fusion.77
  555.8 58.0 %reduce-scatter.4.cloned.1.call-done = f32[3,256,512]{2,1,0:T(8,128)} async-done(((f32[3,256,2048]{2,1,0:T(8,128)}), f32[3,256,512]{2,1,0:T(8,128)}) %reduce-scatter.4.cloned.1.call-update) | async-done | bytes 1572880 | tf_op jit(solution)/shard_map/reduce_scatter | solution.py:44
  618.1 33.8 %collective-permute-done = f32[3,256,512]{2,1,0:T(8,128)S(1)} collective-permute-done((f32[3,256,512]{2,1,0:T(8,128)}, f32[3,256,512]{2,1,0:T(8,128)S(1)}, u32[]{:S(2)}, u32[]{:S(2)}) %collective-permute-start) | collective-permute-done | bytes 1572896 | tf_op jit(solution)/shard_map/ppermute | solution.py:57
  656.9 32.6 %collective-permute-done.1 = f32[3,256,512]{2,1,0:T(8,128)S(1)} collective-permute-done((f32[3,256,512]{2,1,0:T(8,128)S(1)}, f32[3,256,512]{2,1,0:T(8,128)S(1)}, u32[]{:S(2)}, u32[]{:S(2)}) %collective-permute-start.1) | collective-permute-done | bytes 1572896 | tf_op jit(solution)/shard_map/ppermute | solution.py:57
  695.9 31.8 %collective-permute-done.2 = f32[3,256,512]{2,1,0:T(8,128)S(1)} collective-permute-done((f32[3,256,512]{2,1,0:T(8,128)S(1)}, f32[3,256,512]{2,1,0:T(8,128)S(1)}, u32[]{:S(2)}, u32[]{:S(2)}) %collective-permute-start.2) | collective-permute-done | bytes 1572896 | tf_op jit(solution)/shard_map/ppermute | solution.py:57
  732.9 30.9 %collective-permute-done.3 = f32[3,256,512]{2,1,0:T(8,128)S(1)} collective-permute-done((f32[3,256,512]{2,1,0:T(8,128)S(1)}, f32[3,256,512]{2,1,0:T(8,128)S(1)}, u32[]{:S(2)}, u32[]{:S(2)}) %collective-permute-start.3) | collective-permute-done | bytes 1572896 | tf_op jit(solution)/shard_map/ppermute | solution.py:57
  770.1 30.1 %collective-permute-done.4 = f32[3,256,512]{2,1,0:T(8,128)} collective-permute-done((f32[3,256,512]{2,1,0:T(8,128)S(1)}, f32[3,256,512]{2,1,0:T(8,128)}, u32[]{:S(2)}, u32[]{:S(2)}) %collective-permute-start.4) | collective-permute-done | bytes 1572896 | tf_op jit(solution)/shard_map/ppermute | solution.py:57
  800.2 5.3 collective-permute-start.5
  806.2 63.7 %psum.7 = f32[3]{0:T(128)S(1)} all-reduce(f32[3]{0:T(128)S(1)} %pad_maximum_fusion.3), channel_id=1, replica_groups=mesh['fs'=8,'tp'=4] {'fs','tp'}, use_global_device_ids=true, to_apply=%region_2.0 | all-reduce | flops 3 | bytes 24 | tf_op jit(solution)/shard_map/psum | solution.py:32
  890.4 18.5 collective-permute-done.6
  913.3 47.2 %all-gather.20.cloned.1.call-done = f32[3,256,2048]{2,1,0:T(8,128)} async-done(((f32[3,256,512]{2,1,0:T(8,128)}), f32[3,256,2048]{2,1,0:T(8,128)}) %all-gather.20.cloned.1.call-update) | async-done | bytes 6291472 | tf_op jit(solution)/shard_map/all_gather | solution.py:73
  960.4 8.0 fusion.5
  968.5 27.4 fusion
  996.2 45.2 %all-gather.36.cloned.1.call-done = f32[2048,512]{1,0:T(8,128)} async-done(((f32[256,512]{1,0:T(8,128)}), f32[2048,512]{1,0:T(8,128)}) %all-gather.36.cloned.1.call-update) | async-done | bytes 4194320 | tf_op jit(solution)/shard_map/all_gather | solution.py:36
  1041.4 7.3 convolution_bitcast_fusion.1
  1048.7 434.4 %all-gather.22.cloned.1.call-done = f32[2,2048,1408]{2,1,0:T(8,128)} async-done(((f32[2,256,1408]{2,1,0:T(8,128)}), f32[2,2048,1408]{2,1,0:T(8,128)}) %all-gather.22.cloned.1.call-update) | async-done | bytes 23068688 | tf_op jit(solution)/shard_map/all_gather | solution.py:35
  1483.1 24.6 fusion.78
  1510.9 58.0 %reduce-scatter.6.cloned.1.call-done = f32[3,256,512]{2,1,0:T(8,128)} async-done(((f32[3,256,2048]{2,1,0:T(8,128)}), f32[3,256,512]{2,1,0:T(8,128)}) %reduce-scatter.6.cloned.1.call-update) | async-done | bytes 1572880 | tf_op jit(solution)/shard_map/reduce_scatter | solution.py:44
  1573.2 33.7 %collective-permute-done.7 = f32[3,256,512]{2,1,0:T(8,128)} collective-permute-done((f32[3,256,512]{2,1,0:T(8,128)}, f32[3,256,512]{2,1,0:T(8,128)}, u32[]{:S(2)}, u32[]{:S(2)}) %collective-permute-start.7) | collective-permute-done | bytes 1572896 | tf_op jit(solution)/shard_map/ppermute | solution.py:57
  1612.1 32.9 %collective-permute-done.8 = f32[3,256,512]{2,1,0:T(8,128)S(1)} collective-permute-done((f32[3,256,512]{2,1,0:T(8,128)}, f32[3,256,512]{2,1,0:T(8,128)S(1)}, u32[]{:S(2)}, u32[]{:S(2)}) %collective-permute-start.8) | collective-permute-done | bytes 1572896 | tf_op jit(solution)/shard_map/ppermute | solution.py:57
  1651.3 31.8 %collective-permute-done.9 = f32[3,256,512]{2,1,0:T(8,128)S(1)} collective-permute-done((f32[3,256,512]{2,1,0:T(8,128)S(1)}, f32[3,256,512]{2,1,0:T(8,128)S(1)}, u32[]{:S(2)}, u32[]{:S(2)}) %collective-permute-start.9) | collective-permute-done | bytes 1572896 | tf_op jit(solution)/shard_map/ppermute | solution.py:57
  1689.4 30.9 %collective-permute-done.10 = f32[3,256,512]{2,1,0:T(8,128)S(1)} collective-permute-done((f32[3,256,512]{2,1,0:T(8,128)S(1)}, f32[3,256,512]{2,1,0:T(8,128)S(1)}, u32[]{:S(2)}, u32[]{:S(2)}) %collective-permute-start.10) | collective-permute-done | bytes 1572896 | tf_op jit(solution)/shard_map/ppermute | solution.py:57
  1726.6 30.1 %collective-permute-done.11 = f32[3,256,512]{2,1,0:T(8,128)S(1)} collective-permute-done((f32[3,256,512]{2,1,0:T(8,128)S(1)}, f32[3,256,512]{2,1,0:T(8,128)S(1)}, u32[]{:S(2)}, u32[]{:S(2)}) %collective-permute-start.11) | collective-permute-done | bytes 1572896 | tf_op jit(solution)/shard_map/ppermute | solution.py:57
  1763.0 29.2 %collective-permute-done.12 = f32[3,256,512]{2,1,0:T(8,128)} collective-permute-done((f32[3,256,512]{2,1,0:T(8,128)S(1)}, f32[3,256,512]{2,1,0:T(8,128)}, u32[]{:S(2)}, u32[]{:S(2)}) %collective-permute-start.12) | collective-permute-done | bytes 1572896 | tf_op jit(solution)/shard_map/ppermute | solution.py:57
  1792.2 5.5 collective-permute-start.13
  1814.3 12.1 collective-permute-done.13
  1831.5 47.4 %all-gather.26.cloned.1.call-done = f32[3,256,2048]{2,1,0:T(8,128)} async-done(((f32[3,256,512]{2,1,0:T(8,128)}), f32[3,256,2048]{2,1,0:T(8,128)}) %all-gather.26.cloned.1.call-update) | async-done | bytes 6291472 | tf_op jit(solution)/shard_map/all_gather | solution.py:73
  1878.9 7.3 fusion.6
  1886.3 27.4 convolution_add_fusion.1
  1913.9 45.2 %all-gather.38.cloned.1.call-done = f32[2048,512]{1,0:T(8,128)} async-done(((f32[256,512]{1,0:T(8,128)}), f32[2048,512]{1,0:T(8,128)}) %all-gather.38.cloned.1.call-update) | async-done | bytes 4194320 | tf_op jit(solution)/shard_map/all_gather | solution.py:36
  1959.2 7.3 convolution_bitcast_fusion
  1966.5 434.3 %all-gather.28.cloned.1.call-done = f32[2,2048,1408]{2,1,0:T(8,128)} async-done(((f32[2,256,1408]{2,1,0:T(8,128)}), f32[2,2048,1408]{2,1,0:T(8,128)}) %all-gather.28.cloned.1.call-update) | async-done | bytes 23068688 | tf_op jit(solution)/shard_map/all_gather | solution.py:35
  2400.8 24.5 fusion.79
  2428.6 58.0 %reduce-scatter.8.cloned.1.call-done = f32[3,256,512]{2,1,0:T(8,128)} async-done(((f32[3,256,2048]{2,1,0:T(8,128)}), f32[3,256,512]{2,1,0:T(8,128)}) %reduce-scatter.8.cloned.1.call-update) | async-done | bytes 1572880 | tf_op jit(solution)/shard_map/reduce_scatter | solution.py:44
  2490.8 33.7 %collective-permute-done.14 = f32[3,256,512]{2,1,0:T(8,128)} collective-permute-done((f32[3,256,512]{2,1,0:T(8,128)}, f32[3,256,512]{2,1,0:T(8,128)}, u32[]{:S(2)}, u32[]{:S(2)}) %collective-permute-start.14) | collective-permute-done | bytes 1572896 | tf_op jit(solution)/shard_map/ppermute | solution.py:57
  2529.7 32.9 %collective-permute-done.15 = f32[3,256,512]{2,1,0:T(8,128)S(1)} collective-permute-done((f32[3,256,512]{2,1,0:T(8,128)}, f32[3,256,512]{2,1,0:T(8,128)S(1)}, u32[]{:S(2)}, u32[]{:S(2)}) %collective-permute-start.15) | collective-permute-done | bytes 1572896 | tf_op jit(solution)/shard_map/ppermute | solution.py:57
  2568.9 31.8 %collective-permute-done.16 = f32[3,256,512]{2,1,0:T(8,128)S(1)} collective-permute-done((f32[3,256,512]{2,1,0:T(8,128)S(1)}, f32[3,256,512]{2,1,0:T(8,128)S(1)}, u32[]{:S(2)}, u32[]{:S(2)}) %collective-permute-start.16) | collective-permute-done | bytes 1572896 | tf_op jit(solution)/shard_map/ppermute | solution.py:57
  2607.0 30.9 %collective-permute-done.17 = f32[3,256,512]{2,1,0:T(8,128)S(1)} collective-permute-done((f32[3,256,512]{2,1,0:T(8,128)S(1)}, f32[3,256,512]{2,1,0:T(8,128)S(1)}, u32[]{:S(2)}, u32[]{:S(2)}) %collective-permute-start.17) | collective-permute-done | bytes 1572896 | tf_op jit(solution)/shard_map/ppermute | solution.py:57
  2644.3 30.1 %collective-permute-done.18 = f32[3,256,512]{2,1,0:T(8,128)S(1)} collective-permute-done((f32[3,256,512]{2,1,0:T(8,128)S(1)}, f32[3,256,512]{2,1,0:T(8,128)S(1)}, u32[]{:S(2)}, u32[]{:S(2)}) %collective-permute-start.18) | collective-permute-done | bytes 1572896 | tf_op jit(solution)/shard_map/ppermute | solution.py:57
  2680.6 29.2 %collective-permute-done.19 = f32[3,256,512]{2,1,0:T(8,128)} collective-permute-done((f32[3,256,512]{2,1,0:T(8,128)S(1)}, f32[3,256,512]{2,1,0:T(8,128)}, u32[]{:S(2)}, u32[]{:S(2)}) %collective-permute-start.19) | collective-permute-done | bytes 1572896 | tf_op jit(solution)/shard_map/ppermute | solution.py:57
  2709.8 5.5 collective-permute-start.20
  2731.9 12.1 collective-permute-done.20
  2748.9 47.4 %all-gather.32.cloned.1.call-done = f32[3,256,2048]{2,1,0:T(8,128)} async-done(((f32[3,256,512]{2,1,0:T(8,128)}), f32[3,256,2048]{2,1,0:T(8,128)}) %all-gather.32.cloned.1.call-update) | async-done | bytes 6291472 | tf_op jit(solution)/shard_map/all_gather | solution.py:73
  2796.4 7.8 broadcast_multiply_fusion.1
  2804.2 35.0 %broadcast_multiply_fusion = (f32[2,256,1408]{2,1,0:T(8,128)}, f32[2,256,1408]{2,1,0:T(8,128)}) fusion(f32[2,256,1408]{2,1,0:T(8,128)} %param.6, f32[3,256,2048]{2,1,0:T(8,128)S(1)} %copy-done.35, f32[2,2048,1408]{2,1,0:T(8,128)} %all-gather.28.cloned.1.call-done, f32[2,256,1408]{2,1,0:T(8,128)S(1)} %copy-done.2), kind=kOutput, calls=%fused_computation.22 | convolution fusion | flops 17720344576 | bytes 40894464 | tf_op jit(solution)/shard_map/krs,ksc->krc/dot_general | solution.py:75
  (157 shorter events, 182.8 us)
Async XLA Ops:
  7.2 79.1 %all-gather.34.cloned.1.call-start = ((), (), s32[]{:S(2)}) async-start(), calls=%async_computation.15 | async-start | bytes 4718592 | tf_op jit(solution)/shard_map/all_gather | solution.py:36
  9.9 518.0 %all-gather.16.cloned.1.call-start = ((), (), s32[]{:S(2)}) async-start(), calls=%async_computation.3 | async-start | bytes 25952256 | tf_op jit(solution)/shard_map/all_gather | solution.py:35
  14.6 71.6 %copy-start.11 = (f32[256,512]{1,0:T(8,128)S(1)}, f32[256,512]{1,0:T(8,128)}, u32[]{:S(2)}) copy-start(f32[256,512]{1,0:T(8,128)} %get-tuple-element.11) | copy-start | bytes 1572868
  14.6 599.1 %reduce-scatter.4.cloned.1.call-start = ((), (), s32[]{:S(2)}) async-start(), calls=%async_computation.4 | async-start | bytes 7864320 | tf_op jit(solution)/shard_map/reduce_scatter | solution.py:44
  86.2 441.7 %copy-start = (f32[2,256,1408]{2,1,0:T(8,128)S(1)}, f32[2,256,1408]{2,1,0:T(8,128)}, u32[]{:S(2)}) copy-start(f32[2,256,1408]{2,1,0:T(8,128)} %get-tuple-element.9) | copy-start | bytes 8650756
  528.0 24.6 copy-start.8
  555.7 314.2 %all-gather.18.cloned.1.call-start = ((), (), s32[]{:S(2)}) async-start(), calls=%async_computation.5 | async-start | bytes 7864320 | tf_op jit(solution)/shard_map/all_gather | solution.py:45
  613.7 346.7 %all-gather.20.cloned.1.call-start = ((), (), s32[]{:S(2)}) async-start(), calls=%async_computation.6 | async-start | bytes 7864320 | tf_op jit(solution)/shard_map/all_gather | solution.py:73
  613.8 38.1 %collective-permute-start = (f32[3,256,512]{2,1,0:T(8,128)}, f32[3,256,512]{2,1,0:T(8,128)S(1)}, u32[]{:S(2)}, u32[]{:S(2)}) collective-permute-start(f32[3,256,512]{2,1,0:T(8,128)} %reduce-scatter.4.cloned.1.call-done), channel_id=1, source_target_pairs={{0,28},{4,0},{8,4},{12,8},{16,12},{20,16},{24,20},{28,24},{1,29},{... | collective-permute-start | bytes 4718600 | tf_op jit(solution)/shard_map/ppermute | solution.py:57
  651.9 75.8 %copy-start.16 = (f32[3,256,512]{2,1,0:T(8,128)}, f32[3,256,512]{2,1,0:T(8,128)S(1)}, u32[]{:S(2)}) copy-start(f32[3,256,512]{2,1,0:T(8,128)S(1)} %collective-permute-done) | copy-start | bytes 4718596
  651.9 37.7 %collective-permute-start.1 = (f32[3,256,512]{2,1,0:T(8,128)S(1)}, f32[3,256,512]{2,1,0:T(8,128)S(1)}, u32[]{:S(2)}, u32[]{:S(2)}) collective-permute-start(f32[3,256,512]{2,1,0:T(8,128)S(1)} %collective-permute-done), channel_id=1, source_target_pairs={{0,28},{4,0},{8,4},{12,8},{16,12},{20,16},{24,20},{28,24},{1,29},{... | collective-permute-start | bytes 4718600 | tf_op jit(solution)/shard_map/ppermute | solution.py:57
  690.7 37.0 %collective-permute-start.2 = (f32[3,256,512]{2,1,0:T(8,128)S(1)}, f32[3,256,512]{2,1,0:T(8,128)S(1)}, u32[]{:S(2)}, u32[]{:S(2)}) collective-permute-start(f32[3,256,512]{2,1,0:T(8,128)S(1)} %collective-permute-done.1), channel_id=1, source_target_pairs={{0,28},{4,0},{8,4},{12,8},{16,12},{20,16},{24,20},{28,24},{1,29},{... | collective-permute-start | bytes 4718600 | tf_op jit(solution)/shard_map/ppermute | solution.py:57
  727.7 36.1 %collective-permute-start.3 = (f32[3,256,512]{2,1,0:T(8,128)S(1)}, f32[3,256,512]{2,1,0:T(8,128)S(1)}, u32[]{:S(2)}, u32[]{:S(2)}) collective-permute-start(f32[3,256,512]{2,1,0:T(8,128)S(1)} %collective-permute-done.2), channel_id=1, source_target_pairs={{0,28},{4,0},{8,4},{12,8},{16,12},{20,16},{24,20},{28,24},{1,29},{... | collective-permute-start | bytes 4718600 | tf_op jit(solution)/shard_map/ppermute | solution.py:57
  764.9 35.2 %collective-permute-start.4 = (f32[3,256,512]{2,1,0:T(8,128)S(1)}, f32[3,256,512]{2,1,0:T(8,128)}, u32[]{:S(2)}, u32[]{:S(2)}) collective-permute-start(f32[3,256,512]{2,1,0:T(8,128)S(1)} %collective-permute-done.3), channel_id=1, source_target_pairs={{0,28},{4,0},{8,4},{12,8},{16,12},{20,16},{24,20},{28,24},{1,29},{... | collective-permute-start | bytes 4718600 | tf_op jit(solution)/shard_map/ppermute | solution.py:57
  800.2 73.1 %collective-permute-start.5 = (f32[3,256,512]{2,1,0:T(8,128)}, f32[3,256,512]{2,1,0:T(8,128)}, u32[]{:S(2)}, u32[]{:S(2)}) collective-permute-start(f32[3,256,512]{2,1,0:T(8,128)} %collective-permute-done.4), channel_id=1, source_target_pairs={{0,28},{4,0},{8,4},{12,8},{16,12},{20,16},{24,20},{28,24},{1,29},{... | collective-permute-start | bytes 4718600 | tf_op jit(solution)/shard_map/ppermute | solution.py:57
  870.0 9.8 copy-start.12
  873.3 35.6 %collective-permute-start.6 = (f32[3,256,512]{2,1,0:T(8,128)}, f32[3,256,512]{2,1,0:T(8,128)S(1)}, u32[]{:S(2)}, u32[]{:S(2)}) collective-permute-start(f32[3,256,512]{2,1,0:T(8,128)} %collective-permute-done.5), channel_id=1, source_target_pairs={{0,28},{4,0},{8,4},{12,8},{16,12},{20,16},{24,20},{28,24},{1,29},{... | collective-permute-start | bytes 4718600 | tf_op jit(solution)/shard_map/ppermute | solution.py:57
  912.2 129.1 %all-gather.36.cloned.1.call-start = ((), (), s32[]{:S(2)}) async-start(), calls=%async_computation.16 | async-start | bytes 4718592 | tf_op jit(solution)/shard_map/all_gather | solution.py:36
  968.4 514.7 %all-gather.22.cloned.1.call-start = ((), (), s32[]{:S(2)}) async-start(), calls=%async_computation.7 | async-start | bytes 25952256 | tf_op jit(solution)/shard_map/all_gather | solution.py:35
  995.9 45.5 %copy-start.7 = (f32[256,512]{1,0:T(8,128)S(1)}, f32[256,512]{1,0:T(8,128)}, u32[]{:S(2)}) copy-start(f32[256,512]{1,0:T(8,128)} %fusion.5) | copy-start | bytes 1572868
  995.9 572.9 %reduce-scatter.6.cloned.1.call-start = ((), (), s32[]{:S(2)}) async-start(), calls=%async_computation.8 | async-start | bytes 7864320 | tf_op jit(solution)/shard_map/reduce_scatter | solution.py:44
  1041.4 441.7 %copy-start.1 = (f32[2,256,1408]{2,1,0:T(8,128)S(1)}, f32[2,256,1408]{2,1,0:T(8,128)}, u32[]{:S(2)}) copy-start(f32[2,256,1408]{2,1,0:T(8,128)} %fusion) | copy-start | bytes 8650756
  1483.1 24.6 copy-start.9
  1510.9 286.8 %all-gather.24.cloned.1.call-start = ((), (), s32[]{:S(2)}) async-start(), calls=%async_computation.9 | async-start | bytes 7864320 | tf_op jit(solution)/shard_map/all_gather | solution.py:45
  1568.9 38.0 %collective-permute-start.7 = (f32[3,256,512]{2,1,0:T(8,128)}, f32[3,256,512]{2,1,0:T(8,128)}, u32[]{:S(2)}, u32[]{:S(2)}) collective-permute-start(f32[3,256,512]{2,1,0:T(8,128)} %reduce-scatter.6.cloned.1.call-done), channel_id=1, source_target_pairs={{0,28},{4,0},{8,4},{12,8},{16,12},{20,16},{24,20},{28,24},{1,29},{... | collective-permute-start | bytes 4718600 | tf_op jit(solution)/shard_map/ppermute | solution.py:57
  1573.1 305.8 %all-gather.26.cloned.1.call-start = ((), (), s32[]{:S(2)}) async-start(), calls=%async_computation.10 | async-start | bytes 7864320 | tf_op jit(solution)/shard_map/all_gather | solution.py:73
  1606.9 38.1 %collective-permute-start.8 = (f32[3,256,512]{2,1,0:T(8,128)}, f32[3,256,512]{2,1,0:T(8,128)S(1)}, u32[]{:S(2)}, u32[]{:S(2)}) collective-permute-start(f32[3,256,512]{2,1,0:T(8,128)} %collective-permute-done.7), channel_id=1, source_target_pairs={{0,28},{4,0},{8,4},{12,8},{16,12},{20,16},{24,20},{28,24},{1,29},{... | collective-permute-start | bytes 4718600 | tf_op jit(solution)/shard_map/ppermute | solution.py:57
  1646.2 36.9 %collective-permute-start.9 = (f32[3,256,512]{2,1,0:T(8,128)S(1)}, f32[3,256,512]{2,1,0:T(8,128)S(1)}, u32[]{:S(2)}, u32[]{:S(2)}) collective-permute-start(f32[3,256,512]{2,1,0:T(8,128)S(1)} %collective-permute-done.8), channel_id=1, source_target_pairs={{0,28},{4,0},{8,4},{12,8},{16,12},{20,16},{24,20},{28,24},{1,29},{... | collective-permute-start | bytes 4718600 | tf_op jit(solution)/shard_map/ppermute | solution.py:57
  1684.2 36.1 %collective-permute-start.10 = (f32[3,256,512]{2,1,0:T(8,128)S(1)}, f32[3,256,512]{2,1,0:T(8,128)S(1)}, u32[]{:S(2)}, u32[]{:S(2)}) collective-permute-start(f32[3,256,512]{2,1,0:T(8,128)S(1)} %collective-permute-done.9), channel_id=1, source_target_pairs={{0,28},{4,0},{8,4},{12,8},{16,12},{20,16},{24,20},{28,24},{1,29},{... | collective-permute-start | bytes 4718600 | tf_op jit(solution)/shard_map/ppermute | solution.py:57
  1721.4 35.2 %collective-permute-start.11 = (f32[3,256,512]{2,1,0:T(8,128)S(1)}, f32[3,256,512]{2,1,0:T(8,128)S(1)}, u32[]{:S(2)}, u32[]{:S(2)}) collective-permute-start(f32[3,256,512]{2,1,0:T(8,128)S(1)} %collective-permute-done.10), channel_id=1, source_target_pairs={{0,28},{4,0},{8,4},{12,8},{16,12},{20,16},{24,20},{28,24},{1,29},{... | collective-permute-start | bytes 4718600 | tf_op jit(solution)/shard_map/ppermute | solution.py:57
  1757.8 34.4 %collective-permute-start.12 = (f32[3,256,512]{2,1,0:T(8,128)S(1)}, f32[3,256,512]{2,1,0:T(8,128)}, u32[]{:S(2)}, u32[]{:S(2)}) collective-permute-start(f32[3,256,512]{2,1,0:T(8,128)S(1)} %collective-permute-done.11), channel_id=1, source_target_pairs={{0,28},{4,0},{8,4},{12,8},{16,12},{20,16},{24,20},{28,24},{1,29},{... | collective-permute-start | bytes 4718600 | tf_op jit(solution)/shard_map/ppermute | solution.py:57
  1792.2 34.1 %collective-permute-start.13 = (f32[3,256,512]{2,1,0:T(8,128)}, f32[3,256,512]{2,1,0:T(8,128)}, u32[]{:S(2)}, u32[]{:S(2)}) collective-permute-start(f32[3,256,512]{2,1,0:T(8,128)} %collective-permute-done.12), channel_id=1, source_target_pairs={{0,28},{4,0},{8,4},{12,8},{16,12},{20,16},{24,20},{28,24},{1,29},{... | collective-permute-start | bytes 4718600 | tf_op jit(solution)/shard_map/ppermute | solution.py:57
  1831.5 127.7 %all-gather.38.cloned.1.call-start = ((), (), s32[]{:S(2)}) async-start(), calls=%async_computation.17 | async-start | bytes 4718592 | tf_op jit(solution)/shard_map/all_gather | solution.py:36
  1886.2 514.5 %all-gather.28.cloned.1.call-start = ((), (), s32[]{:S(2)}) async-start(), calls=%async_computation.11 | async-start | bytes 25952256 | tf_op jit(solution)/shard_map/all_gather | solution.py:35
  1913.7 45.5 %copy-start.6 = (f32[256,512]{1,0:T(8,128)S(1)}, f32[256,512]{1,0:T(8,128)}, u32[]{:S(2)}) copy-start(f32[256,512]{1,0:T(8,128)} %fusion.6) | copy-start | bytes 1572868
  1913.7 572.8 %reduce-scatter.8.cloned.1.call-start = ((), (), s32[]{:S(2)}) async-start(), calls=%async_computation.12 | async-start | bytes 7864320 | tf_op jit(solution)/shard_map/reduce_scatter | solution.py:44
  1959.2 441.6 %copy-start.2 = (f32[2,256,1408]{2,1,0:T(8,128)S(1)}, f32[2,256,1408]{2,1,0:T(8,128)}, u32[]{:S(2)}) copy-start(f32[2,256,1408]{2,1,0:T(8,128)} %convolution_add_fusion.1) | copy-start | bytes 8650756
  2400.8 24.6 copy-start.10
  2428.5 286.8 %all-gather.30.cloned.1.call-start = ((), (), s32[]{:S(2)}) async-start(), calls=%async_computation.13 | async-start | bytes 7864320 | tf_op jit(solution)/shard_map/all_gather | solution.py:45
  2486.5 38.0 %collective-permute-start.14 = (f32[3,256,512]{2,1,0:T(8,128)}, f32[3,256,512]{2,1,0:T(8,128)}, u32[]{:S(2)}, u32[]{:S(2)}) collective-permute-start(f32[3,256,512]{2,1,0:T(8,128)} %reduce-scatter.8.cloned.1.call-done), channel_id=1, source_target_pairs={{0,28},{4,0},{8,4},{12,8},{16,12},{20,16},{24,20},{28,24},{1,29},{... | collective-permute-start | bytes 4718600 | tf_op jit(solution)/shard_map/ppermute | solution.py:57
  2490.8 305.6 %all-gather.32.cloned.1.call-start = ((), (), s32[]{:S(2)}) async-start(), calls=%async_computation.14 | async-start | bytes 7864320 | tf_op jit(solution)/shard_map/all_gather | solution.py:73
  2524.6 38.1 %collective-permute-start.15 = (f32[3,256,512]{2,1,0:T(8,128)}, f32[3,256,512]{2,1,0:T(8,128)S(1)}, u32[]{:S(2)}, u32[]{:S(2)}) collective-permute-start(f32[3,256,512]{2,1,0:T(8,128)} %collective-permute-done.14), channel_id=1, source_target_pairs={{0,28},{4,0},{8,4},{12,8},{16,12},{20,16},{24,20},{28,24},{1,29},{... | collective-permute-start | bytes 4718600 | tf_op jit(solution)/shard_map/ppermute | solution.py:57
  2563.8 36.8 %collective-permute-start.16 = (f32[3,256,512]{2,1,0:T(8,128)S(1)}, f32[3,256,512]{2,1,0:T(8,128)S(1)}, u32[]{:S(2)}, u32[]{:S(2)}) collective-permute-start(f32[3,256,512]{2,1,0:T(8,128)S(1)} %collective-permute-done.15), channel_id=1, source_target_pairs={{0,28},{4,0},{8,4},{12,8},{16,12},{20,16},{24,20},{28,24},{1,29},{... | collective-permute-start | bytes 4718600 | tf_op jit(solution)/shard_map/ppermute | solution.py:57
  2601.8 36.1 %collective-permute-start.17 = (f32[3,256,512]{2,1,0:T(8,128)S(1)}, f32[3,256,512]{2,1,0:T(8,128)S(1)}, u32[]{:S(2)}, u32[]{:S(2)}) collective-permute-start(f32[3,256,512]{2,1,0:T(8,128)S(1)} %collective-permute-done.16), channel_id=1, source_target_pairs={{0,28},{4,0},{8,4},{12,8},{16,12},{20,16},{24,20},{28,24},{1,29},{... | collective-permute-start | bytes 4718600 | tf_op jit(solution)/shard_map/ppermute | solution.py:57
  2639.1 35.2 %collective-permute-start.18 = (f32[3,256,512]{2,1,0:T(8,128)S(1)}, f32[3,256,512]{2,1,0:T(8,128)S(1)}, u32[]{:S(2)}, u32[]{:S(2)}) collective-permute-start(f32[3,256,512]{2,1,0:T(8,128)S(1)} %collective-permute-done.17), channel_id=1, source_target_pairs={{0,28},{4,0},{8,4},{12,8},{16,12},{20,16},{24,20},{28,24},{1,29},{... | collective-permute-start | bytes 4718600 | tf_op jit(solution)/shard_map/ppermute | solution.py:57
  2675.5 34.4 %collective-permute-start.19 = (f32[3,256,512]{2,1,0:T(8,128)S(1)}, f32[3,256,512]{2,1,0:T(8,128)}, u32[]{:S(2)}, u32[]{:S(2)}) collective-permute-start(f32[3,256,512]{2,1,0:T(8,128)S(1)} %collective-permute-done.18), channel_id=1, source_target_pairs={{0,28},{4,0},{8,4},{12,8},{16,12},{20,16},{24,20},{28,24},{1,29},{... | collective-permute-start | bytes 4718600 | tf_op jit(solution)/shard_map/ppermute | solution.py:57
  2709.8 34.1 %collective-permute-start.20 = (f32[3,256,512]{2,1,0:T(8,128)}, f32[3,256,512]{2,1,0:T(8,128)}, u32[]{:S(2)}, u32[]{:S(2)}) collective-permute-start(f32[3,256,512]{2,1,0:T(8,128)} %collective-permute-done.19), channel_id=1, source_target_pairs={{0,28},{4,0},{8,4},{12,8},{16,12},{20,16},{24,20},{28,24},{1,29},{... | collective-permute-start | bytes 4718600 | tf_op jit(solution)/shard_map/ppermute | solution.py:57
  2796.4 7.8 copy-start.35
  (24 other events, 58.7 us)
Sparse Core Ops, SparseCore 0:
  10.7 75.5 all-gather.33
  88.3 439.5 all-gather.15
  555.8 57.8 reduce-scatter.3
  615.1 46.3 all-gather.17
  912.3 48.0 all-gather.19
  968.5 72.7 all-gather.35
  1043.5 439.5 all-gather.21
  1511.0 57.8 reduce-scatter.5
  1573.2 43.5 all-gather.23
  1831.6 47.2 all-gather.25
  1886.4 72.7 all-gather.37
  1961.2 439.5 all-gather.27
  2428.6 57.8 reduce-scatter.7
  2490.9 43.3 all-gather.29
  2749.1 47.2 all-gather.31
